TPU v7x, 512 devices: a whole 4x4x16 slice. The times are simulated.
512 devices in a mesh: ep: 32 (over z, core), tp: 16 (over y, x).
Axes of the slice: x: 4, y: 4, z: 16, core: 2. Of those that a mesh axis runs over, the one named last changes fastest.
Arguments:
- query_rows: bfloat16 [12288, 2048], P('ep', 'tp'), may hold values from -6 to 6
- key_rows: bfloat16 [12288, 2048], P('ep', 'tp'), may hold values from -6 to 6
- value_rows: bfloat16 [12288, 2048], P('ep', 'tp'), may hold values from -6 to 6
- second_scale: float32 [16], P('tp'), may hold values from 0.3 to 0.8
- head_gain: float32 [128], replicated, may hold values from 0.1 to 1.9
- out_weight: bfloat16 [2048, 4096], P(None, 'tp'), may hold values from -0.125 to 0.125
- routed_rows: bfloat16 [4096, 4096], P('ep', 'tp'), may hold values from -6 to 6
- norm_gain: float32 [4096], replicated, may hold values from 0.1 to 1.9
- route_ids: int32 [4096, 2], P('ep'), may hold values from 0 to 31, all different within a row; in each aligned block of 128 rows (0 to 127, 128 to 255, ...) at most 16 rows name the same one
- route_weight: float32 [4096, 2], P('ep'), may hold values from 0.1 to 0.9
- expert_gate: bfloat16 [32, 4096, 2048], P('ep', None, 'tp'), may hold values from -0.09375 to 0.09375
- expert_up: bfloat16 [32, 4096, 2048], P('ep', None, 'tp'), may hold values from -0.09375 to 0.09375
- expert_down: bfloat16 [32, 2048, 4096], P('ep', None, 'tp'), may hold values from -0.125 to 0.125
Outputs:
- mixer_out: bfloat16 [12288, 4096], P('ep', 'tp')
- expert_mix: bfloat16 [4096, 4096], P('ep', 'tp')
Inputs may be any that keep to these rules, and one draw needn't show every extreme that they name: `route_ids`: among the 128 tokens of one index of ep, no expert is named by more than 16 of them, a bound that some block reaches.
All inputs are finite; a program needn't handle non-finite values.
Results may differ from a plain program's by a relative error of at most 0.0085.
Values may be sent and summed in bfloat16 or wider, within the bound.
A program may use at most 64 MiB of HBM per device.

v0:
```python
import jax
import jax.numpy as jnp
from jax import lax
from jax.sharding import PartitionSpec as P

eps = 1e-06
head_factor = 0.8
neg_big = -1e30
key_block_rows = 1024


def side_by_side(arrays, axis, dim, along):
    both = jnp.concatenate(arrays, axis=along)
    result, at, finished = (lax.all_gather(both, axis, axis=dim, tiled=True), 0, [])
    for a in arrays:
        finished.append(lax.slice_in_dim(result, at, at + a.shape[along], axis=along))
        at += a.shape[along]
    return tuple(finished)


def rms_rows(rows_in, gain):
    floats = rows_in.astype(jnp.float32)
    factor = lax.rsqrt(jnp.mean(floats * floats, axis=-1, keepdims=True) + eps)
    return (floats * factor * gain).astype(jnp.bfloat16)


def per_device(
    query_rows,
    key_rows,
    value_rows,
    second_scale,
    head_gain,
    out_weight,
    routed_rows,
    norm_gain,
    route_ids,
    route_weight,
    expert_gate,
    expert_up,
    expert_down,
):
    count_a = query_rows.shape[0]
    per_head = second_scale.shape[0]
    head_dim = query_rows.shape[1] // (2 * per_head)
    value_dim = head_gain.shape[0]
    query_four = query_rows.reshape(count_a, per_head, 2, head_dim)
    query_pos = lax.axis_index("ep") * count_a + jnp.arange(count_a, dtype=jnp.int32)

    def key_block(carry_state, key_part, value_part, block_start):
        key_count = key_part.shape[0]
        key_four = key_part.reshape(key_count, per_head, 2, head_dim)
        value_three = value_part.reshape(key_count, per_head, value_dim)
        scores = jnp.einsum(
            "ihcd,jhcd->ihcj", query_four, key_four, preferred_element_type=jnp.float32
        ) * head_dim ** (-0.5)
        allowed = (
            query_pos[:, None] >= block_start + jnp.arange(key_count, dtype=jnp.int32)[None, :]
        )[:, None, None, :]
        scores = jnp.where(allowed, scores, neg_big)
        old_max, old_sum, old_acc = carry_state
        new_max = jnp.maximum(old_max, jnp.max(scores, axis=-1))
        weights = jnp.where(allowed, jnp.exp(scores - new_max[..., None]), 0.0)
        shrink = jnp.exp(old_max - new_max)
        new_sum = old_sum * shrink + jnp.sum(weights, axis=-1)
        update = jnp.einsum(
            "ihcj,jhe->ihce",
            weights.astype(jnp.bfloat16),
            value_three,
            preferred_element_type=jnp.float32,
        )
        return (new_max, new_sum, old_acc * shrink[..., None] + update)

    start_state = (
        jnp.full((count_a, per_head, 2), neg_big, jnp.float32),
        jnp.zeros((count_a, per_head, 2), jnp.float32),
        jnp.zeros((count_a, per_head, 2, value_dim), jnp.float32),
    )
    key_part, value_part = side_by_side((key_rows, value_rows), "ep", 0, 1)
    key_count = key_part.shape[0]

    def step_block(block_num, inner_state):
        offset_rows = block_num * key_block_rows
        key_slice = lax.dynamic_slice_in_dim(key_part, offset_rows, key_block_rows, 0)
        value_slice = lax.dynamic_slice_in_dim(value_part, offset_rows, key_block_rows, 0)
        return key_block(inner_state, key_slice, value_slice, offset_rows)

    run_max, run_sum, run_acc = lax.fori_loop(
        0, key_count // key_block_rows, step_block, start_state
    )
    maps_both = run_acc / run_sum[..., None]
    mixed_maps = maps_both[:, :, 0] - second_scale[None, :, None] * maps_both[:, :, 1]
    mean_sq = jnp.mean(mixed_maps * mixed_maps, axis=-1, keepdims=True)
    head_out = (
        (mixed_maps * lax.rsqrt(mean_sq + eps) * head_gain * head_factor)
        .astype(jnp.bfloat16)
        .reshape(count_a, per_head * value_dim)
    )
    count_b = routed_rows.shape[0]
    route_count = route_ids.shape[1]
    experts_here = expert_gate.shape[0]
    ep_devices = lax.axis_size("ep")
    expert_total = experts_here * ep_devices
    capacity = 2 * count_b * route_count // expert_total
    flat_expert = route_ids.reshape(-1)
    chosen = (flat_expert[:, None] == jnp.arange(expert_total, dtype=jnp.int32)[None, :]).astype(
        jnp.int32
    )
    ranks = jnp.sum((jnp.cumsum(chosen, axis=0) - 1) * chosen, axis=1)
    slot_of = flat_expert * capacity + ranks
    token_of = jnp.arange(count_b * route_count, dtype=jnp.int32) // route_count
    slot_token = jnp.full((expert_total * capacity,), count_b, jnp.int32).at[slot_of].set(token_of)
    padded = jnp.concatenate(
        [routed_rows, jnp.zeros((1, routed_rows.shape[1]), jnp.bfloat16)], axis=0
    )
    outgoing = padded[slot_token].reshape(ep_devices, experts_here, capacity, routed_rows.shape[1])
    column_parts = lax.all_to_all(outgoing, "ep", split_axis=0, concat_axis=0, tiled=True)
    arrived = rms_rows(lax.all_gather(column_parts, "tp", axis=3, tiled=True), norm_gain)
    gate_val = jnp.einsum(
        "sxcd,xdf->sxcf", arrived, expert_gate, preferred_element_type=jnp.float32
    )
    up_val = jnp.einsum("sxcd,xdf->sxcf", arrived, expert_up, preferred_element_type=jnp.float32)
    hidden = (jax.nn.silu(gate_val) * up_val).astype(jnp.bfloat16)
    weight_rows = out_weight
    attn_total = jnp.dot(
        lax.all_gather(
            head_out.reshape(1, 1, count_a, head_out.shape[1]), "tp", axis=3, tiled=True
        )[0, 0],
        weight_rows,
        preferred_element_type=jnp.float32,
    )
    weight_rows = expert_down
    moe_total = jnp.einsum(
        "sxcf,xfd->sxcd",
        lax.all_gather(hidden, "tp", axis=3, tiled=True),
        weight_rows,
        preferred_element_type=jnp.float32,
    )
    mixer_out = attn_total.astype(jnp.bfloat16)
    returned = lax.all_to_all(
        moe_total.astype(jnp.bfloat16), "ep", split_axis=0, concat_axis=0, tiled=True
    )
    flat_back = returned.reshape(expert_total * capacity, returned.shape[3])
    picked = flat_back[slot_of].astype(jnp.float32).reshape(count_b, route_count, returned.shape[3])
    expert_mix = jnp.sum(picked * route_weight[:, :, None], axis=1).astype(jnp.bfloat16)
    return (mixer_out, expert_mix)


def solution(mesh):
    placed = (
        P("ep", "tp"),
        P("ep", "tp"),
        P("ep", "tp"),
        P("tp"),
        P(),
        P(None, "tp"),
        P("ep", "tp"),
        P(),
        P("ep", None),
        P("ep", None),
        P("ep", None, "tp"),
        P("ep", None, "tp"),
        P("ep", None, "tp"),
    )
    return jax.shard_map(
        per_device,
        mesh=mesh,
        in_specs=placed,
        out_specs=(P("ep", "tp"), P("ep", "tp")),
        check_vma=False,
    )
```

profile of v0, /device:TPU:32, one launch (start us, length us, event | category | flops | bytes accessed | tf_op | source)
XLA Modules:
  0.0 361.6 jit_solution(12429718926275836795)
XLA Ops:
  14.6 36.4 %all_to_all.10 = bf16[32,1,16,256]{3,2,1,0:T(8,128)(2,1)} all-to-all(bf16[32,1,16,256]{3,2,1,0:T(8,128)(2,1)S(1)} %bitcast.173), channel_id=1, replica_groups=mesh['ep'=32,'tp'=16] {'ep'}, dimensions={0} | all-to-all | bytes 524288 | tf_op jit(solution)/shard_map/all_to_all | solution.py:116
  52.9 63.2 %all-gather.9.cloned.1.call-done = bf16[32,1,16,4096]{3,2,1,0:T(8,128)(2,1)} async-done(((bf16[32,1,16,256]{3,2,1,0:T(8,128)(2,1)}), bf16[32,1,16,4096]{3,2,1,0:T(8,128)(2,1)}) %all-gather.9.cloned.1.call-update) | async-done | bytes 4194320 | tf_op jit(solution)/shard_map/all_gather | solution.py:117
  116.0 3.2 fusion.24
  122.8 71.9 %all-gather.5.cloned.1.call-done = bf16[12288,256]{0,1:T(8,128)(2,1)} async-done(((bf16[384,256]{0,1:T(8,128)(2,1)}), bf16[12288,256]{0,1:T(8,128)(2,1)}) %all-gather.5.cloned.1.call-update) | async-done | bytes 6291472 | tf_op jit(solution)/shard_map/all_gather | solution.py:14
  194.7 6.2 %fusion.69 = (bf16[12288,128]{0,1:T(8,128)(2,1)}, bf16[12288,128]{0,1:T(8,128)(2,1)}) fusion(bf16[12288,256]{0,1:T(8,128)(2,1)} %all-gather.5.cloned.1.call-done), kind=kLoop, calls=%fused_computation.86 | loop fusion | bytes 12582912 | tf_op jit(solution)/shard_map/slice | solution.py:16
  200.9 94.7 %while.18 = (s32[]{:T(128)}, f32[384,1,2]{0,2,1:T(2,128)S(1)}, f32[384,1,2]{0,2,1:T(2,128)S(1)}, f32[384,1,2,128]{0,3,2,1:T(8,128)S(1)}, bf16[12288,128]{0,1:T(8...) while((s32[]{:T(128)}, f32[384,1,2]{0,2,1:T(2,128)S(1)}, ...), condition=%wide.region_3.4_spmd.clone, body=%wide.region_0.3_spmd.clone.sunk | while | flops 312907648 | bytes 25586904 | solution.py:87
  204.6 3.2 fusion.85
  212.5 3.2 fusion.85
  220.4 3.2 fusion.85
  228.3 3.2 fusion.85
  236.2 3.2 fusion.85
  241.6 2.4 fusion.82
  244.1 3.2 fusion.85
  252.0 3.3 fusion.85
  259.9 3.2 fusion.85
  267.8 3.2 fusion.85
  275.7 3.2 fusion.85
  283.6 3.2 fusion.85
  291.5 3.2 fusion.85
  296.5 3.1 fusion.48
  299.6 8.2 %all-to-all-start.1 = ((bf16[32,1,16,256]{3,2,1,0:T(8,128)(2,1)}), bf16[32,1,16,256]{3,2,1,0:T(8,128)(2,1)S(1)}, u32[]{:S(2)}, u32[]{:S(2)}) async-start(bf16[32,1,16,256]{3,2,1,0:T(8,128)(2,1)} %fusion.48), calls=%async_computation.1 | async-start | bytes 524288 | tf_op jit(solution)/shard_map/all_to_all | solution.py:139
  308.0 20.8 %all-to-all-done.1 = bf16[32,1,16,256]{3,2,1,0:T(8,128)(2,1)S(1)} async-done(((bf16[32,1,16,256]{3,2,1,0:T(8,128)(2,1)}), bf16[32,1,16,256]{3,2,1,0:T(8,128)(2,1)S(1)}, u32[]{:S(2)}, u32[]{:S(2)}) %all-to-all-start.1) | async-done | bytes 262176 | tf_op jit(solution)/shard_map/all_to_all | solution.py:139
  331.1 21.2 %all-gather.7.cloned.1.call-done = bf16[1,1,384,2048]{2,3,1,0:T(8,128)(2,1)} async-done(((bf16[1,1,384,128]{2,3,1,0:T(8,128)(2,1)}), bf16[1,1,384,2048]{2,3,1,0:T(8,128)(2,1)}) %all-gather.7.cloned.1.call-update) | async-done | bytes 1572880 | tf_op jit(solution)/shard_map/all_gather | solution.py:125
  352.4 2.7 fusion.39
  (200 shorter events, 67.8 us)
Async XLA Ops:
  7.2 289.4 %copy-start = (bf16[1,2048,256]{2,1,0:T(8,128)(2,1)S(1)}, bf16[1,2048,256]{2,1,0:T(8,128)(2,1)}, u32[]{:S(2)}) copy-start(bf16[1,2048,256]{2,1,0:T(8,128)(2,1)} %param.27) | copy-start | bytes 3145732
  7.2 43.8 %copy-start.4 = (bf16[384,128]{1,0:T(8,128)(2,1)S(1)}, bf16[384,128]{1,0:T(8,128)(2,1)}, u32[]{:S(2)}) copy-start(bf16[384,128]{1,0:T(8,128)(2,1)} %param.16) | copy-start | bytes 294916
  7.2 43.9 %copy-start.5 = (bf16[384,128]{1,0:T(8,128)(2,1)S(1)}, bf16[384,128]{1,0:T(8,128)(2,1)}, u32[]{:S(2)}) copy-start(bf16[384,128]{1,0:T(8,128)(2,1)} %param.17) | copy-start | bytes 294916
  7.2 44.9 %copy-start.6 = (bf16[384,128]{1,0:T(8,128)(2,1)S(1)}, bf16[384,128]{1,0:T(8,128)(2,1)}, u32[]{:S(2)}) copy-start(bf16[384,128]{1,0:T(8,128)(2,1)} %param.15) | copy-start | bytes 294916
  7.2 108.8 %all-gather.9.cloned.1.call-start = ((), (), s32[]{:S(2)}) async-start(), calls=%async_computation.4 | async-start | bytes 4456448 | tf_op jit(solution)/shard_map/all_gather | solution.py:117
  14.5 104.7 %copy-start.9 = (bf16[1,4096,128]{2,1,0:T(8,128)(2,1)S(1)}, bf16[1,4096,128]{2,1,0:T(8,128)(2,1)}, u32[]{:S(2)}) copy-start(bf16[1,4096,128]{2,1,0:T(8,128)(2,1)} %param.25) | copy-start | bytes 3145732
  14.5 104.7 %copy-start.11 = (f32[4096]{0:T(1024)S(1)}, f32[4096]{0:T(1024)}, u32[]{:S(2)}) copy-start(f32[4096]{0:T(1024)} %param.22) | copy-start | bytes 49156
  50.9 143.8 %all-gather.5.cloned.1.call-start = ((), (), s32[]{:S(2)}) async-start(), calls=%async_computation.2 | async-start | bytes 6488064 | tf_op jit(solution)/shard_map/all_gather | solution.py:14
  52.0 244.5 %all-gather.11.cloned.1.call-start = ((), (), s32[]{:S(2)}) async-start(), calls=%async_computation.5 | async-start | bytes 2228224 | tf_op jit(solution)/shard_map/all_gather | solution.py:134
  116.0 3.4 copy-start.2
  122.8 229.6 %all-gather.7.cloned.1.call-start = ((), (), s32[]{:S(2)}) async-start(), calls=%async_computation.3 | async-start | bytes 1671168 | tf_op jit(solution)/shard_map/all_gather | solution.py:125
  200.9 94.8 %copy-start.8 = (f32[128]{0:T(128)S(1)}, f32[128]{0:T(128)}, u32[]{:S(2)}) copy-start(f32[128]{0:T(128)} %param.19) | copy-start | bytes 1540
  212.5 3.3 copy-start.1
  220.4 3.3 copy-start.1
  228.3 3.3 copy-start.1
  236.2 3.3 copy-start.1
  252.0 3.3 copy-start.1
  267.8 3.3 copy-start.1
  275.7 3.3 copy-start.1
  283.6 3.3 copy-start.1
  291.5 3.3 copy-start.1
  295.6 12.3 %copy-start.7 = (f32[128,2]{0,1:T(2,128)S(1)}, f32[128,2]{0,1:T(2,128)}, u32[]{:S(2)}) copy-start(f32[128,2]{0,1:T(2,128)} %param.24) | copy-start | bytes 3076
  296.5 55.9 %copy-start.3 = (bf16[2048,256]{1,0:T(8,128)(2,1)S(1)}, bf16[2048,256]{1,0:T(8,128)(2,1)}, u32[]{:S(2)}) copy-start(bf16[2048,256]{1,0:T(8,128)(2,1)} %param.20) | copy-start | bytes 3145732
  299.6 29.2 %all-to-all-start.1 = ((bf16[32,1,16,256]{3,2,1,0:T(8,128)(2,1)}), bf16[32,1,16,256]{3,2,1,0:T(8,128)(2,1)S(1)}, u32[]{:S(2)}, u32[]{:S(2)}) async-start(bf16[32,1,16,256]{3,2,1,0:T(8,128)(2,1)} %fusion.48), calls=%async_computation.1 | async-start | bytes 524288 | tf_op jit(solution)/shard_map/all_to_all | solution.py:139
  (4 other events, 11.1 us)
Sparse Core Ops, SparseCore 0:
  51.1 64.9 all-gather.8
  118.7 75.9 all-gather.4
  197.7 59.0 all-gather.10
  296.6 55.7 all-gather.6
where the time goes:
time: 362 us
  waiting for transfers between devices  177 us (49%)
  matrix products  77 us (21%)
  blocking collectives  36.4 us (10%)
  local copies, waits for them, and re-layouts  25.7 us (7%)
  other arithmetic  21.3 us (6%)
  between operations  14.7 us (4%)
  starting transfers between devices  8.4 us (2%)
    all_gather x1, waiting for transfers between devices, side_by_side(): lax.all_gather(both, axis, axis=dim, tiled=True)  71.9 us
    all_gather x1, waiting for transfers between devices, per_device(): lax.all_gather(column_parts, 'tp', axis=3, tiled=True)  63.2 us
    dot_general x12, matrix products, key_block(): jnp.einsum('ihcj,jhe->ihce', weights.astype(jnp.bfloat16), value_three, p...  38.8 us
    all_to_all x1, blocking collectives, per_device(): lax.all_to_all(outgoing, 'ep', split_axis=0, concat_axis=0, tiled=True)  36.4 us
    dot_general x12, matrix products, key_block(): jnp.einsum('ihcd,jhcd->ihcj', query_four, key_four, preferred_element_typ...  29.1 us
    all_gather x1, waiting for transfers between devices, per_device(): lax.all_gather(head_out.reshape(1, 1, count_a, head_out.shape[1]), 'tp',...  21.2 us
    all_to_all x1, waiting for transfers between devices, per_device(): lax.all_to_all(moe_total.astype(jnp.bfloat16), 'ep', split_axis=0, concat...  20.8 us
    dynamic_slice x12, local copies, waits for them, and re-layouts, step_block(): lax.dynamic_slice_in_dim(key_part, offset_rows, key_block_rows, 0)  11.7 us
  transfers between devices with their start and end apart: 5, of which 4 were waited for; matrix products, arithmetic and copies ran while one was open for 31% of the time, Pallas kernels for 0%

commit v1 on v0

--- a/solution.py
+++ b/solution.py
@@ -7,6 +7,18 @@
 head_factor = 0.8
 neg_big = -1e30
 key_block_rows = 1024
+
+
+def gather_by_bits(x, axis, dim):
+    ways, here, step = (lax.axis_size(axis), lax.axis_index(axis), x.shape[dim])
+    line, have = (x, 1)
+    while have < ways:
+        line = jnp.concatenate(
+            [line, lax.ppermute(line, axis, [(d, (d - have) % ways) for d in range(ways)])],
+            axis=dim,
+        )
+        have = 2 * have
+    return jnp.roll(line, here * step, axis=dim)
 
 
 def side_by_side(arrays, axis, dim, along):
@@ -114,7 +126,7 @@
     )
     outgoing = padded[slot_token].reshape(ep_devices, experts_here, capacity, routed_rows.shape[1])
     column_parts = lax.all_to_all(outgoing, "ep", split_axis=0, concat_axis=0, tiled=True)
-    arrived = rms_rows(lax.all_gather(column_parts, "tp", axis=3, tiled=True), norm_gain)
+    arrived = rms_rows(gather_by_bits(column_parts, "tp", 3), norm_gain)
     gate_val = jnp.einsum(
         "sxcd,xdf->sxcf", arrived, expert_gate, preferred_element_type=jnp.float32
     )

time: 362 us -> 338 us (0.934)
  waiting for transfers between devices: 177 us -> 121 us
  starting transfers between devices: 8.4 us -> 30.2 us
  local copies, waits for them, and re-layouts: 25.7 us -> 32.8 us
    ppermute x0 -> x4, waiting for transfers between devices: none -> 76 us  [gather_by_bits(): lax.ppermute(line, axis, [(d, (d - have) % ways) for d in range(ways)])]
    all_gather x1, waiting for transfers between devices: 71.9 us -> 0.02 us  [side_by_side(): lax.all_gather(both, axis, axis=dim, tiled=True)]
    all_gather x1 -> x0, waiting for transfers between devices: 63.2 us -> none  [per_device(): lax.all_gather(column_parts, 'tp', axis=3, tiled=True)]
    ppermute x0 -> x4, starting transfers between devices: none -> 17.8 us  [gather_by_bits(): lax.ppermute(line, axis, [(d, (d - have) % ways) for d in range(ways)])]
    unnamed x27 -> x30, local copies, waits for them, and re-layouts: 1.6 us -> 6.83 us
    all_to_all x1, starting transfers between devices: 8.23 us -> 12.2 us  [per_device(): lax.all_to_all(moe_total.astype(jnp.bfloat16), 'ep', split_axis=0, concat...]
  transfers between devices with their start and end apart: 5 -> 8, of which waited for: 4 -> 6; matrix products, arithmetic and copies ran while one was open for 31% -> 37% of each run, Pallas kernels for 0% -> 0%
where the time goes in v1:
time: 338 us; the launch traced here: 337 us
  waiting for transfers between devices  121 us (36%)
  matrix products  77.1 us (23%)
  blocking collectives  39.7 us (12%)
  local copies, waits for them, and re-layouts  32.8 us (10%)
  starting transfers between devices  30.2 us (9%)
  other arithmetic  20.7 us (6%)
  between operations  14.8 us (4%)
    ppermute x4, waiting for transfers between devices, gather_by_bits(): lax.ppermute(line, axis, [(d, (d - have) % ways) for d in range(ways)])  76 us
    all_to_all x1, blocking collectives, per_device(): lax.all_to_all(outgoing, 'ep', split_axis=0, concat_axis=0, tiled=True)  39.7 us
    dot_general x12, matrix products, key_block(): jnp.einsum('ihcj,jhe->ihce', weights.astype(jnp.bfloat16), value_three, p...  38.9 us
    dot_general x12, matrix products, key_block(): jnp.einsum('ihcd,jhcd->ihcj', query_four, key_four, preferred_element_typ...  29.3 us
    all_gather x1, waiting for transfers between devices, per_device(): lax.all_gather(head_out.reshape(1, 1, count_a, head_out.shape[1]), 'tp',...  24.3 us
    all_to_all x1, waiting for transfers between devices, per_device(): lax.all_to_all(moe_total.astype(jnp.bfloat16), 'ep', split_axis=0, concat...  20.8 us
    ppermute x4, starting transfers between devices, gather_by_bits(): lax.ppermute(line, axis, [(d, (d - have) % ways) for d in range(ways)])  17.8 us
    all_to_all x1, starting transfers between devices, per_device(): lax.all_to_all(moe_total.astype(jnp.bfloat16), 'ep', split_axis=0, concat...  12.2 us
  transfers between devices with their start and end apart: 8, of which 6 were waited for; matrix products, arithmetic and copies ran while one was open for 37% of the time, Pallas kernels for 0%

profile of v1, /device:TPU:32, one launch (start us, length us, event | category | flops | bytes accessed | tf_op | source)
XLA Modules:
  0.0 337.4 jit_solution(11104766812872295247)
XLA Ops:
  17.3 39.7 %all_to_all.10 = bf16[32,1,16,256]{3,2,1,0:T(8,128)(2,1)S(1)} all-to-all(bf16[32,1,16,256]{3,2,1,0:T(8,128)(2,1)S(1)} %bitcast.171), channel_id=1, replica_groups=mesh['ep'=32,'tp'=16] {'ep'}, dimensions={0} | all-to-all | bytes 524288 | tf_op jit(solution)/shard_map/all_to_all | solution.py:128
  57.0 6.8 %collective-permute-start = (bf16[32,1,16,256]{3,2,1,0:T(8,128)(2,1)S(1)}, bf16[32,1,16,256]{3,2,1,0:T(8,128)(2,1)S(1)}, u32[]{:S(2)}, u32[]{:S(2)}) collective-permute-start(bf16[32,1,16,256]{3,2,1,0:T(8,128)(2,1)S(1)} %all_to_all.10), channel_id=1, source_target_pairs={{0,15},{1,0},{2,1},{3,2},{4,3},{5,4},{6,5},{7,6},{8,7},{9,8},{10,9... | collective-permute-start | bytes 786440 | tf_op jit(solution)/shard_map/ppermute | solution.py:17
  63.8 4.1 %collective-permute-done = bf16[32,1,16,256]{3,2,1,0:T(8,128)(2,1)S(1)} collective-permute-done((bf16[32,1,16,256]{3,2,1,0:T(8,128)(2,1)S(1)}, bf16[32,1,16,256]{3,2,1,0:T(8,128)(2,1)S(1)}, u32[]{:S(2)}, u32[]{:S(2)}) %collective-permute-start) | collective-permute-done | bytes 262176 | tf_op jit(solution)/shard_map/ppermute | solution.py:17
  68.0 4.7 %collective-permute-start.1 = (bf16[32,1,16,512]{3,2,1,0:T(8,128)(2,1)S(1)}, bf16[32,1,16,512]{3,2,1,0:T(8,128)(2,1)S(1)}, u32[]{:S(2)}, u32[]{:S(2)}) collective-permute-start(bf16[32,1,16,512]{3,2,1,0:T(8,128)(2,1)S(1)} %pad_maximum_fusion.2), channel_id=1, source_target_pairs={{0,14},{1,15},{2,0},{3,1},{4,2},{5,3},{6,4},{7,5},{8,6},{9,7},{10,... | collective-permute-start | bytes 1572872 | tf_op jit(solution)/shard_map/ppermute | solution.py:17
  72.7 10.1 %collective-permute-done.1 = bf16[32,1,16,512]{3,2,1,0:T(8,128)(2,1)S(1)} collective-permute-done((bf16[32,1,16,512]{3,2,1,0:T(8,128)(2,1)S(1)}, bf16[32,1,16,512]{3,2,1,0:T(8,128)(2,1)S(1)}, u32[]{:S(2)}, u32[]{:S(2)}) %collective-permute-start.1) | collective-permute-done | bytes 524320 | tf_op jit(solution)/shard_map/ppermute | solution.py:17
  85.8 20.8 %collective-permute-done.2 = bf16[32,1,16,1024]{3,2,1,0:T(8,128)(2,1)S(1)} collective-permute-done((bf16[32,1,16,1024]{3,2,1,0:T(8,128)(2,1)S(1)}, bf16[32,1,16,1024]{3,2,1,0:T(8,128)(2,1)S(1)}, u32[]{:S(2)}, u32[]{:S(2)}) %collective-permute-start.2) | collective-permute-done | bytes 1048608 | tf_op jit(solution)/shard_map/ppermute | solution.py:17
  108.1 3.4 %collective-permute-start.3 = (bf16[32,1,16,2048]{3,2,1,0:T(8,128)(2,1)}, bf16[32,1,16,2048]{3,2,1,0:T(8,128)(2,1)}, u32[]{:S(2)}, u32[]{:S(2)}) collective-permute-start(bf16[32,1,16,2048]{3,2,1,0:T(8,128)(2,1)} %pad_maximum_fusion), channel_id=1, source_target_pairs={{0,8},{1,9},{2,10},{3,11},{4,12},{5,13},{6,14},{7,15},{8,0},{9,1},... | collective-permute-start | bytes 6291464 | tf_op jit(solution)/shard_map/ppermute | solution.py:17
  114.1 41.1 %collective-permute-done.3 = bf16[32,1,16,2048]{3,2,1,0:T(8,128)(2,1)} collective-permute-done((bf16[32,1,16,2048]{3,2,1,0:T(8,128)(2,1)}, bf16[32,1,16,2048]{3,2,1,0:T(8,128)(2,1)}, u32[]{:S(2)}, u32[]{:S(2)}) %collective-permute-start.3) | collective-permute-done | bytes 2097184 | tf_op jit(solution)/shard_map/ppermute | solution.py:17
  163.5 6.2 %fusion.69 = (bf16[12288,128]{0,1:T(8,128)(2,1)}, bf16[12288,128]{0,1:T(8,128)(2,1)}) fusion(bf16[12288,256]{0,1:T(8,128)(2,1)} %all-gather.4.cloned.1.call-done), kind=kLoop, calls=%fused_computation.100 | loop fusion | bytes 12582912 | tf_op jit(solution)/shard_map/slice | solution.py:28
  169.7 94.8 %while.18 = (s32[]{:T(128)}, f32[384,1,2]{0,2,1:T(2,128)S(1)}, f32[384,1,2]{0,2,1:T(2,128)S(1)}, f32[384,1,2,128]{0,3,2,1:T(8,128)S(1)}, bf16[12288,128]{0,1:T(8...) while((s32[]{:T(128)}, f32[384,1,2]{0,2,1:T(2,128)S(1)}, ...), condition=%wide.region_3.4_spmd.clone, body=%wide.region_0.3_spmd.clone.sunk | while | flops 312907648 | bytes 25586904 | solution.py:99
  173.4 3.2 fusion.85
  181.3 3.2 fusion.85
  189.2 3.3 fusion.85
  205.1 3.2 fusion.85
  212.9 3.3 fusion.85
  220.9 3.2 fusion.85
  228.8 3.2 fusion.85
  236.7 3.2 fusion.85
  244.6 3.2 fusion.85
  252.5 3.2 fusion.85
  260.4 3.2 fusion.85
  268.4 12.2 %all-to-all-start.1 = ((bf16[32,1,16,256]{3,2,1,0:T(8,128)(2,1)}), bf16[32,1,16,256]{3,2,1,0:T(8,128)(2,1)S(1)}, u32[]{:S(2)}, u32[]{:S(2)}) async-start(bf16[32,1,16,256]{3,2,1,0:T(8,128)(2,1)} %fusion.48), calls=%async_computation.1 | async-start | bytes 524288 | tf_op jit(solution)/shard_map/all_to_all | solution.py:151
  280.7 20.8 %all-to-all-done.1 = bf16[32,1,16,256]{3,2,1,0:T(8,128)(2,1)S(1)} async-done(((bf16[32,1,16,256]{3,2,1,0:T(8,128)(2,1)}), bf16[32,1,16,256]{3,2,1,0:T(8,128)(2,1)S(1)}, u32[]{:S(2)}, u32[]{:S(2)}) %all-to-all-start.1) | async-done | bytes 262176 | tf_op jit(solution)/shard_map/all_to_all | solution.py:151
  303.9 24.3 %all-gather.6.cloned.1.call-done = bf16[1,1,384,2048]{2,3,1,0:T(8,128)(2,1)} async-done(((bf16[1,1,384,128]{2,3,1,0:T(8,128)(2,1)}), bf16[1,1,384,2048]{2,3,1,0:T(8,128)(2,1)}) %all-gather.6.cloned.1.call-update) | async-done | bytes 1572880 | tf_op jit(solution)/shard_map/all_gather | solution.py:137
  (212 shorter events, 92.0 us)
Async XLA Ops:
  7.2 258.3 %copy-start = (bf16[1,2048,256]{2,1,0:T(8,128)(2,1)S(1)}, bf16[1,2048,256]{2,1,0:T(8,128)(2,1)}, u32[]{:S(2)}) copy-start(bf16[1,2048,256]{2,1,0:T(8,128)(2,1)} %param.27) | copy-start | bytes 3145732
  7.2 156.3 %all-gather.4.cloned.1.call-start = ((), (), s32[]{:S(2)}) async-start(), calls=%async_computation.2 | async-start | bytes 6488064 | tf_op jit(solution)/shard_map/all_gather | solution.py:26
  10.1 255.4 %all-gather.8.cloned.1.call-start = ((), (), s32[]{:S(2)}) async-start(), calls=%async_computation.4 | async-start | bytes 2228224 | tf_op jit(solution)/shard_map/all_gather | solution.py:146
  57.0 10.9 %collective-permute-start = (bf16[32,1,16,256]{3,2,1,0:T(8,128)(2,1)S(1)}, bf16[32,1,16,256]{3,2,1,0:T(8,128)(2,1)S(1)}, u32[]{:S(2)}, u32[]{:S(2)}) collective-permute-start(bf16[32,1,16,256]{3,2,1,0:T(8,128)(2,1)S(1)} %all_to_all.10), channel_id=1, source_target_pairs={{0,15},{1,0},{2,1},{3,2},{4,3},{5,4},{6,5},{7,6},{8,7},{9,8},{10,9... | collective-permute-start | bytes 786440 | tf_op jit(solution)/shard_map/ppermute | solution.py:17
  68.0 14.8 %collective-permute-start.1 = (bf16[32,1,16,512]{3,2,1,0:T(8,128)(2,1)S(1)}, bf16[32,1,16,512]{3,2,1,0:T(8,128)(2,1)S(1)}, u32[]{:S(2)}, u32[]{:S(2)}) collective-permute-start(bf16[32,1,16,512]{3,2,1,0:T(8,128)(2,1)S(1)} %pad_maximum_fusion.2), channel_id=1, source_target_pairs={{0,14},{1,15},{2,0},{3,1},{4,2},{5,3},{6,4},{7,5},{8,6},{9,7},{10,... | collective-permute-start | bytes 1572872 | tf_op jit(solution)/shard_map/ppermute | solution.py:17
  82.9 23.6 %collective-permute-start.2 = (bf16[32,1,16,1024]{3,2,1,0:T(8,128)(2,1)S(1)}, bf16[32,1,16,1024]{3,2,1,0:T(8,128)(2,1)S(1)}, u32[]{:S(2)}, u32[]{:S(2)}) collective-permute-start(bf16[32,1,16,1024]{3,2,1,0:T(8,128)(2,1)S(1)} %pad_maximum_fusion.1), channel_id=1, source_target_pairs={{0,12},{1,13},{2,14},{3,15},{4,0},{5,1},{6,2},{7,3},{8,4},{9,5},{1... | collective-permute-start | bytes 3145736 | tf_op jit(solution)/shard_map/ppermute | solution.py:17
  108.1 47.1 %collective-permute-start.3 = (bf16[32,1,16,2048]{3,2,1,0:T(8,128)(2,1)}, bf16[32,1,16,2048]{3,2,1,0:T(8,128)(2,1)}, u32[]{:S(2)}, u32[]{:S(2)}) collective-permute-start(bf16[32,1,16,2048]{3,2,1,0:T(8,128)(2,1)} %pad_maximum_fusion), channel_id=1, source_target_pairs={{0,8},{1,9},{2,10},{3,11},{4,12},{5,13},{6,14},{7,15},{8,0},{9,1},... | collective-permute-start | bytes 6291464 | tf_op jit(solution)/shard_map/ppermute | solution.py:17
  163.3 6.4 %copy-start.3 = (bf16[384,128]{0,1:T(8,128)(2,1)S(1)}, bf16[384,128]{0,1:T(8,128)(2,1)}, u32[]{:S(2)}) copy-start(bf16[384,128]{0,1:T(8,128)(2,1)} %copy.32) | copy-start | bytes 294916
  163.3 164.9 %all-gather.6.cloned.1.call-start = ((), (), s32[]{:S(2)}) async-start(), calls=%async_computation.3 | async-start | bytes 1671168 | tf_op jit(solution)/shard_map/all_gather | solution.py:137
  169.7 94.9 %copy-start.5 = (f32[128]{0:T(128)S(1)}, f32[128]{0:T(128)}, u32[]{:S(2)}) copy-start(f32[128]{0:T(128)} %param.19) | copy-start | bytes 1540
  173.4 3.3 copy-start.1
  181.3 3.3 copy-start.1
  189.2 3.3 copy-start.1
  205.0 3.3 copy-start.1
  212.9 3.3 copy-start.1
  220.9 3.3 copy-start.1
  228.8 3.3 copy-start.1
  236.7 3.3 copy-start.1
  244.6 3.3 copy-start.1
  252.4 3.3 copy-start.1
  260.3 3.3 copy-start.1
  264.5 16.1 %copy-start.4 = (f32[128,2]{0,1:T(2,128)S(1)}, f32[128,2]{0,1:T(2,128)}, u32[]{:S(2)}) copy-start(f32[128,2]{0,1:T(2,128)} %param.24) | copy-start | bytes 3076
  264.5 63.7 %copy-start.2 = (bf16[2048,256]{1,0:T(8,128)(2,1)S(1)}, bf16[2048,256]{1,0:T(8,128)(2,1)}, u32[]{:S(2)}) copy-start(bf16[2048,256]{1,0:T(8,128)(2,1)} %param.20) | copy-start | bytes 3145732
  268.4 33.1 %all-to-all-start.1 = ((bf16[32,1,16,256]{3,2,1,0:T(8,128)(2,1)}), bf16[32,1,16,256]{3,2,1,0:T(8,128)(2,1)S(1)}, u32[]{:S(2)}, u32[]{:S(2)}) async-start(bf16[32,1,16,256]{3,2,1,0:T(8,128)(2,1)} %fusion.48), calls=%async_computation.1 | async-start | bytes 524288 | tf_op jit(solution)/shard_map/all_to_all | solution.py:151
  (4 other events, 10.1 us)
Sparse Core Ops, SparseCore 0:
  10.6 88.9 all-gather.3
  163.4 65.9 all-gather.7
  265.5 62.6 all-gather.5
